TPU v7x, 128 devices: a whole 4x4x4 slice. The times are simulated.
128 devices in a mesh: rep: 2 (over z_hi), fs: 32 (over z_lo, y, x), tp: 2 (over core).
Axes of the slice: x: 4, y: 4, z: 4 (z_hi: 2, z_lo: 2; z = z_hi * 2 + z_lo), core: 2. Of those that a mesh axis runs over, the one named last changes fastest.
Arguments:
- tokens: bfloat16 [65536, 2048], P(('rep', 'fs', 'tp')), may hold values from -6 to 6
- pre_gain: bfloat16 [2048], replicated, may hold values from 0.099609375 to 1.8984375
- gate_weight: bfloat16 [2048, 2816], P('fs', 'tp'), may hold values from -0.125 to 0.125
- value_weight: bfloat16 [2048, 2816], P('fs', 'tp'), may hold values from -0.125 to 0.125
- down_weight: bfloat16 [2816, 2048], P('tp', 'fs'), may hold values from -0.109375 to 0.109375
- post_gain: bfloat16 [2048], replicated, may hold values from 0.099609375 to 1.8984375
Outputs:
- updated: bfloat16 [65536, 2048], P(('rep', 'fs', 'tp'))
All inputs are finite; a program needn't handle non-finite values.
Results may differ from a plain program's by a relative error of at most 0.0055.
Values may be sent and summed in bfloat16 or wider, within the bound.
No kernel may reach another device: no remote copies, remote signals or barrier semaphores. Data moves between devices by JAX's collectives and lax.ppermute only.
A program may use at most 128 MiB of HBM per device.

v0:
```python
import jax
import jax.numpy as jnp
from jax import lax
from jax.sharding import Mesh
from jax.sharding import PartitionSpec as P

FS = ("fs_0", "fs_1", "fs_2")
REP_FS_TP = ("rep", "fs_0", "fs_1", "fs_2", "tp")


eps_norm = 1e-06


def in_order(parts, dim):
    lengths = list(parts.shape[1:])
    lengths[dim] *= parts.shape[0]
    return jnp.moveaxis(parts, 0, dim).reshape(lengths)


def sent_to_all(array, axis):
    peers = lax.axis_size(axis)
    return lax.all_to_all(
        jnp.broadcast_to(array[None], (peers, *array.shape)), axis, 0, 0, tiled=True
    )


def gathered_copies(array, axis, dim):
    return in_order(sent_to_all(array, axis), dim)


def in_one_piece(arrays, axis, dim, along):
    both = jnp.concatenate(arrays, axis=along)
    whole, at, finished = (lax.all_gather(both, axis, axis=dim, tiled=True), 0, [])
    for a in arrays:
        finished.append(lax.slice_in_dim(whole, at, at + a.shape[along], axis=along))
        at += a.shape[along]
    return tuple(finished)


def gather_in_order(array, axes, turns):
    parts = array
    for k in turns:
        parts = lax.all_gather(parts, axes[k])
    done = turns[::-1]
    back = [done.index(k) for k in range(len(axes))]
    parts = parts.transpose(*back, *range(len(axes), parts.ndim))
    return parts.reshape(-1, *array.shape)


def gathered_by_axis(array, axes, turns, dim):
    return in_order(gather_in_order(array, axes, turns), dim)


def cut_along(array, dim, peers):
    lengths = array.shape
    parts = array.reshape(*lengths[:dim], peers, lengths[dim] // peers, *lengths[dim + 1 :])
    return jnp.moveaxis(parts, dim, 0)


def sent_and_summed(array, axis, dim):
    parts = cut_along(array, dim, lax.axis_size(axis))
    arrived = lax.all_to_all(parts, axis, split_axis=0, concat_axis=0, tiled=True)
    return arrived.astype(jnp.float32).sum(axis=0)


def rms_rows(values_in, gain):
    floats = values_in.astype(jnp.float32)
    scaled = floats * lax.rsqrt(jnp.mean(floats * floats, -1, keepdims=True) + eps_norm)
    return scaled * gain.astype(jnp.float32)


def shards(tokens, pre_gain, gate_weight, value_weight, down_weight, post_gain):
    normed = rms_rows(tokens, pre_gain).astype(jnp.bfloat16)
    group_rows = gathered_copies(normed, "tp", 0)
    pieces = in_one_piece((gate_weight, value_weight), FS, 0, 1)
    gate_add = jnp.dot(group_rows, pieces[0], preferred_element_type=jnp.float32)
    value_add = jnp.dot(group_rows, pieces[1], preferred_element_type=jnp.float32)
    down_full = gathered_by_axis(down_weight, FS, (0, 1, 2), 1)
    hidden = (jax.nn.silu(gate_add) * value_add).astype(jnp.bfloat16)
    branch = sent_and_summed(
        jnp.dot(hidden, down_full, preferred_element_type=jnp.float32).astype(jnp.bfloat16), "tp", 0
    ).astype(jnp.bfloat16)
    updated = tokens.astype(jnp.float32) + 0.5 * rms_rows(branch, post_gain)
    return updated.astype(jnp.bfloat16)


def solution(mesh):
    torus = Mesh(
        mesh.devices.reshape(mesh.shape["rep"], 2, 4, 4, mesh.shape["tp"]),
        ("rep", "fs_0", "fs_1", "fs_2", "tp"),
    )
    in_specs = (P(REP_FS_TP, None), P(), P(FS, "tp"), P(FS, "tp"), P("tp", FS), P())
    out_specs = P(REP_FS_TP, None)
    return jax.shard_map(
        shards, mesh=torus, in_specs=in_specs, out_specs=out_specs, check_vma=False
    )
```

profile of v0, /device:TPU:1, one launch (start us, length us, event | category | flops | bytes accessed | tf_op | source)
XLA Modules:
  0.0 340.0 jit_solution(4226136508492825143)
XLA Ops:
  6.5 7.8 %all-gather = bf16[2816,64]{0,1:T(8,128)(2,1)S(1)} all-gather(bf16[1408,64]{0,1:T(8,128)(2,1)} %param.10), channel_id=2, replica_groups=mesh['rep'=2,'fs_0'=2,'fs_1'=4,'fs_2'=4,'tp'=2] {'fs_0'}, dimensions={0}, use_global_device_ids=true | all-gather | bytes 540672 | tf_op jit(solution)/shard_map/all_gather | solution.py:43
  14.3 0.8 copy.14
  15.1 0.0 all-gather.9.cloned.1.call-update
  15.1 0.0 all-gather.11.cloned.1.call-start
  15.1 28.1 %all-gather.9.cloned.1.call-done = bf16[8,1408,64]{1,2,0:T(8,128)(2,1)} async-done(((bf16[2,1408,64]{1,2,0:T(8,128)(2,1)}), bf16[8,1408,64]{1,2,0:T(8,128)(2,1)}) %all-gather.9.cloned.1.call-update) | async-done | bytes 1441808 | tf_op jit(solution)/shard_map/all_gather | solution.py:43
  43.2 0.0 all-gather.11.cloned.1.call-update
  43.2 0.0 all-gather.7.cloned.1.call-start
  43.3 1.8 pad_maximum_fusion
  45.0 0.0 all-gather.7.cloned.1.call-update
  45.1 0.7 convert_element_type.28
  45.8 0.5 fusion.12
  46.3 0.6 fusion.14
  46.8 2.6 broadcast_in_dim.2
  49.4 6.6 %all-to-all-start = ((bf16[2,512,2048]{2,1,0:T(8,128)(2,1)}), bf16[2,512,2048]{2,1,0:T(8,128)(2,1)}, u32[]{:S(2)}, u32[]{:S(2)}) async-start(bf16[2,512,2048]{2,1,0:T(8,128)(2,1)} %broadcast_in_dim.2), calls=%async_computation | async-start | bytes 8388608 | tf_op jit(solution)/shard_map/all_to_all | solution.py:22
  56.0 50.5 %all-gather.11.cloned.1.call-done = bf16[16,2,1408,64]{2,3,1,0:T(8,128)(2,1)} async-done(((bf16[4,2,1408,64]{2,3,1,0:T(8,128)(2,1)}), bf16[16,2,1408,64]{2,3,1,0:T(8,128)(2,1)}) %all-gather.11.cloned.1.call-update) | async-done | bytes 5767184 | tf_op jit(solution)/shard_map/all_gather | solution.py:43
  106.5 5.7 %copy.11 = bf16[2,4,4,1408,64]{3,4,2,1,0:T(8,128)(2,1)} copy(bf16[2,4,4,1408,64]{3,4,0,1,2:T(8,128)(2,1)} %bitcast.18) | data formatting | bytes 11534336 | tf_op jit(solution)/shard_map/transpose | solution.py:46
  112.2 0.0 all-to-all-done
  112.2 149.4 %all-gather.7.cloned.1.call-done = bf16[2048,2816]{1,0:T(8,128)(2,1)} async-done(((bf16[64,2816]{1,0:T(8,128)(2,1)}), bf16[2048,2816]{1,0:T(8,128)(2,1)}) %all-gather.7.cloned.1.call-update) | async-done | bytes 11534352 | tf_op jit(solution)/shard_map/all_gather | solution.py:33
  261.6 11.7 %fusion.2 = f32[1024,1408]{1,0:T(8,128)} fusion(bf16[1024,2048]{1,0:T(8,128)(2,1)} %bitcast, bf16[2048,2816]{1,0:T(8,128)(2,1)} %all-gather.7.cloned.1.call-done), kind=kOutput, calls=%fused_computation.5 | convolution fusion | flops 5905580032 | bytes 15728640 | tf_op jit(solution)/shard_map/dot_general | solution.py:76
  273.3 20.6 %fusion.16 = bf16[1024,2048]{1,0:T(8,128)(2,1)} fusion(bf16[1408,2048]{0,1:T(8,128)(2,1)} %bitcast.19, f32[1024,1408]{1,0:T(8,128)} %fusion.2, bf16[1024,2048]{1,0:T(8,128)(2,1)} %bitcast, bf16[2048,2816]{1,0:T(8,128)(2,1)} %all-gather.7.cloned.1.call-done), kind=kOutput, calls=%fused_computation.18 | convolution fusion | flops 11821907968 | bytes 25690112 | tf_op jit(solution)/shard_map/dot_general | solution.py:81
  293.9 31.5 %all_to_all.10 = bf16[2,512,2048]{2,1,0:T(8,128)(2,1)} all-to-all(bf16[2,512,2048]{2,1,0:T(8,128)(2,1)} %bitcast.20), channel_id=1, replica_groups=mesh['rep'=2,'fs_0'=2,'fs_1'=4,'fs_2'=4,'tp'=2] {'tp'}, dimensions={0} | all-to-all | bytes 8388608 | tf_op jit(solution)/shard_map/all_to_all | solution.py:62
  325.4 3.4 reduce_sum.31
  328.8 0.5 fusion.9
  329.3 4.2 %fusion.15 = bf16[512,2048]{1,0:T(8,128)(2,1)} fusion(bf16[512,2048]{1,0:T(8,128)(2,1)S(1)} %reduce_sum.31, bf16[512,2048]{1,0:T(8,128)(2,1)} %param.6, f32[2048]{0:T(1024)S(1)} %convert_element_type.33, f32[512]{0:T(512)S(1)} %add_rsqrt_fusion), kind=kLoop, calls=%fused_computation.17 | loop fusion | flops 7340032 | bytes 6301696 | tf_op jit(solution)/shard_map/convert_element_type | solution.py:84
  (8 shorter events, 0.0 us)
Async XLA Ops:
  6.5 39.2 %copy-start = (bf16[512,2048]{1,0:T(8,128)(2,1)S(1)}, bf16[512,2048]{1,0:T(8,128)(2,1)}, u32[]{:S(2)}) copy-start(bf16[512,2048]{1,0:T(8,128)(2,1)} %param.6) | copy-start | bytes 6291460
  6.5 36.7 %all-gather.9.cloned.1.call-start = ((), (), s32[]{:S(2)}) async-start(), calls=%async_computation.3 | async-start | bytes 1802240 | tf_op jit(solution)/shard_map/all_gather | solution.py:43
  15.1 91.4 %all-gather.11.cloned.1.call-start = ((), (), s32[]{:S(2)}) async-start(), calls=%async_computation.4 | async-start | bytes 7208960 | tf_op jit(solution)/shard_map/all_gather | solution.py:43
  43.2 218.4 %all-gather.7.cloned.1.call-start = ((), (), s32[]{:S(2)}) async-start(), calls=%async_computation.2 | async-start | bytes 11894784 | tf_op jit(solution)/shard_map/all_gather | solution.py:33
  49.4 6.6 %copy-start.1 = (bf16[2048]{0:T(1024)(128)(2,1)S(1)}, bf16[2048]{0:T(1024)(128)(2,1)}, u32[]{:S(2)}) copy-start(bf16[2048]{0:T(1024)(128)(2,1)} %param.11) | copy-start | bytes 12292
  49.4 62.7 %all-to-all-start = ((bf16[2,512,2048]{2,1,0:T(8,128)(2,1)}), bf16[2,512,2048]{2,1,0:T(8,128)(2,1)}, u32[]{:S(2)}, u32[]{:S(2)}) async-start(bf16[2,512,2048]{2,1,0:T(8,128)(2,1)} %broadcast_in_dim.2), calls=%async_computation | async-start | bytes 8388608 | tf_op jit(solution)/shard_map/all_to_all | solution.py:22
Sparse Core Ops, SparseCore 0:
  15.2 27.9 all-gather.8
  44.9 61.5 all-gather.10
  108.1 153.3 all-gather.6
where the time goes:
time: 341 us; the launch traced here: 340 us
  waiting for transfers between devices  228 us (67%)
  blocking collectives  39.3 us (12%)
  matrix products  32.3 us (9%)
  between operations  13.1 us (4%)
  other arithmetic  11.6 us (3%)
  local copies, waits for them, and re-layouts  9.03 us (3%)
  starting transfers between devices  6.64 us (2%)
    all_gather x1, waiting for transfers between devices, in_one_piece(): lax.all_gather(both, axis, axis=dim, tiled=True)  149 us
    all_gather x2, waiting for transfers between devices, gather_in_order(): parts = lax.all_gather(parts, axes[k])  78.6 us
    all_to_all x1, blocking collectives, sent_and_summed(): lax.all_to_all(parts, axis, split_axis=0, concat_axis=0, tiled=True)  31.5 us
    dot_general x1, matrix products, shards(): jnp.dot(hidden, down_full, preferred_element_type=jnp.float32)  20.6 us
    dot_general x1, matrix products, shards(): jnp.dot(group_rows, pieces[0], preferred_element_type=jnp.float32)  11.7 us
    all_gather x1, blocking collectives, gather_in_order(): parts = lax.all_gather(parts, axes[k])  7.76 us
  transfers between devices with their start and end apart: 4, of which 3 were waited for; matrix products, arithmetic and copies ran while one was open for 3% of the time, Pallas kernels for 0%

commit v1 on v0

v1 whole, which is shorter than its diff:
```python
import jax
import jax.numpy as jnp
from jax import lax
from jax.sharding import Mesh
from jax.sharding import PartitionSpec as P

FS = ("fs_0", "fs_1", "fs_2")
REP_FS = ("rep", "fs_0", "fs_1", "fs_2")
REP_FS_TP = ("rep", "fs_0", "fs_1", "fs_2", "tp")

eps_norm = 1e-06
SWAP = [(0, 1), (1, 0)]


def rms_rows(values_in, gain):
    floats = values_in.astype(jnp.float32)
    scaled = floats * lax.rsqrt(jnp.mean(floats * floats, -1, keepdims=True) + eps_norm)
    return scaled * gain.astype(jnp.float32)


def shards(tokens, pre_gain, gate_weight, value_weight, down_weight, post_gain):
    rep = lax.axis_index("rep")
    down_rows = down_weight.T
    half = down_rows.shape[0] // 2
    own = jnp.where(rep == 0, gate_weight, value_weight)
    own_down = lax.dynamic_slice_in_dim(down_rows, rep * half, half, 0)
    sent = jnp.concatenate([own, own_down], 0)
    rows = own.shape[0]
    whole = lax.all_gather(sent, REP_FS, axis=0)
    whole = whole.reshape(2, -1, *sent.shape)
    gate = whole[0, :, :rows].reshape(-1, sent.shape[1])
    value = whole[1, :, :rows].reshape(-1, sent.shape[1])
    down = whole[:, :, rows:].swapaxes(0, 1).reshape(-1, sent.shape[1])

    normed = rms_rows(tokens, pre_gain).astype(jnp.bfloat16)
    other = lax.ppermute(normed, "tp", SWAP)

    def partial(rows_in):
        gate_add = jnp.dot(rows_in, gate, preferred_element_type=jnp.float32)
        value_add = jnp.dot(rows_in, value, preferred_element_type=jnp.float32)
        hidden = (jax.nn.silu(gate_add) * value_add).astype(jnp.bfloat16)
        return lax.dot_general(
            hidden, down, (((1,), (1,)), ((), ())), preferred_element_type=jnp.float32
        ).astype(jnp.bfloat16)

    theirs = lax.ppermute(partial(other), "tp", SWAP)
    mine = partial(normed)
    branch = (mine.astype(jnp.float32) + theirs.astype(jnp.float32)).astype(jnp.bfloat16)
    updated = tokens.astype(jnp.float32) + 0.5 * rms_rows(branch, post_gain)
    return updated.astype(jnp.bfloat16)


def solution(mesh):
    torus = Mesh(
        mesh.devices.reshape(mesh.shape["rep"], 2, 4, 4, mesh.shape["tp"]),
        ("rep", "fs_0", "fs_1", "fs_2", "tp"),
    )
    in_specs = (P(REP_FS_TP, None), P(), P(FS, "tp"), P(FS, "tp"), P("tp", FS), P())
    out_specs = P(REP_FS_TP, None)
    return jax.shard_map(
        shards, mesh=torus, in_specs=in_specs, out_specs=out_specs, check_vma=False
    )
```

time: 341 us -> 191 us (0.56)
  waiting for transfers between devices: 228 us -> 103 us
  blocking collectives: 39.3 us -> 0 us
  matrix products: 32.3 us -> 44.9 us
  local copies, waits for them, and re-layouts: 9.03 us -> 16.7 us
  starting transfers between devices: 6.64 us -> 2.22 us
    all_gather x3 -> x1, waiting for transfers between devices: 228 us -> 103 us  [shards(): whole = lax.all_gather(sent, REP_FS, axis=0)]
    all_to_all x1 -> x0, blocking collectives: 31.5 us -> none  [sent_and_summed(): lax.all_to_all(parts, axis, split_axis=0, concat_axis=0, tiled=True)]
    dot_general x2 -> x4, matrix products: 32.3 us -> 44.9 us  [the longest x2 28.4 us: partial(): lax.dot_general(hidden, down, (((1,), (1,)), ((), ())), preferred_element...]
    slice x0 -> x1, local copies, waits for them, and re-layouts: none -> 9.44 us  [shards(): gate = whole[0, :, :rows].reshape(-1, sent.shape[1])]
    all_gather x1 -> x0, blocking collectives: 7.76 us -> none  [gather_in_order(): parts = lax.all_gather(parts, axes[k])]
    all_to_all x1 -> x0, starting transfers between devices: 6.56 us -> none  [sent_to_all(): lax.all_to_all(jnp.broadcast_to(array[None], (peers, *array.shape)), axis...]
  transfers between devices with their start and end apart: 4 -> 3, of which waited for: 3 -> 1; matrix products, arithmetic and copies ran while one was open for 3% -> 15% of each run, Pallas kernels for 0% -> 0%
where the time goes in v1:
time: 191 us
  waiting for transfers between devices  103 us (54%)
  matrix products  44.9 us (24%)
  local copies, waits for them, and re-layouts  16.7 us (9%)
  between operations  13.4 us (7%)
  other arithmetic  10.5 us (5%)
  starting transfers between devices  2.22 us (1%)
    all_gather x1, waiting for transfers between devices, shards(): whole = lax.all_gather(sent, REP_FS, axis=0)  103 us
    dot_general x2, matrix products, partial(): lax.dot_general(hidden, down, (((1,), (1,)), ((), ())), preferred_element...  28.4 us
    dot_general x2, matrix products, partial(): gate_add = jnp.dot(rows_in, gate, preferred_element_type=jnp.float32)  16.5 us
    slice x1, local copies, waits for them, and re-layouts, shards(): gate = whole[0, :, :rows].reshape(-1, sent.shape[1])  9.44 us
    transpose x2, local copies, waits for them, and re-layouts, shards(): down = whole[:, :, rows:].swapaxes(0, 1).reshape(-1, sent.shape[1])  6.34 us
    convert_element_type x1, other arithmetic, shards(): return updated.astype(jnp.bfloat16)  4.17 us
  transfers between devices with their start and end apart: 3, of which 1 were waited for; matrix products, arithmetic and copies ran while one was open for 15% of the time, Pallas kernels for 0%

profile of v1, /device:TPU:1, one launch (start us, length us, event | category | flops | bytes accessed | tf_op | source)
XLA Modules:
  0.0 191.0 jit_solution(11502384226029344727)
XLA Ops:
  6.5 0.0 copy-start
  6.5 0.0 all-gather.3.cloned.1.call-start
  6.5 0.9 copy-done
  7.5 1.0 broadcast_select_fusion
  8.4 0.7 pad_maximum_fusion
  9.2 0.0 all-gather.3.cloned.1.call-update
  9.2 0.7 convert_element_type.41
  9.9 2.1 %fusion.3 = f32[512]{0:T(512)S(1)} fusion(bf16[512,2048]{1,0:T(8,128)(2,1)} %param.6), kind=kLoop, calls=%fused_computation.9 | loop fusion | flops 3145216 | bytes 2099200 | tf_op jit(solution)/shard_map/reduce_sum | solution.py:17
  12.0 0.0 copy-done.1
  12.0 1.9 fusion.5
  13.8 1.4 collective-permute-start
  15.2 103.2 %all-gather.3.cloned.1.call-done = bf16[6144,1408]{1,0:T(8,128)(2,1)} async-done(((bf16[96,1408]{1,0:T(8,128)(2,1)}), bf16[6144,1408]{1,0:T(8,128)(2,1)}) %all-gather.3.cloned.1.call-update) | async-done | bytes 17301520 | tf_op jit(solution)/shard_map/all_gather | solution.py:29
  118.4 3.1 %slice_bitcast_fusion = bf16[32,2,32,1408]{3,2,0,1:T(8,128)(2,1)S(1)} fusion(bf16[2,32,96,1408]{3,2,1,0:T(8,128)(2,1)} %bitcast.18), kind=kLoop, calls=%fused_computation.3 | loop fusion | bytes 11534336 | tf_op jit(solution)/shard_map/transpose | solution.py:33
  121.5 3.3 %copy.7 = bf16[32,2,32,1408]{3,2,1,0:T(8,128)(2,1)} copy(bf16[32,2,32,1408]{3,2,0,1:T(8,128)(2,1)S(1)} %slice_bitcast_fusion) | data formatting | bytes 11534336 | tf_op jit(solution)/shard_map/transpose | solution.py:33
  124.8 9.4 %fusion.11 = (bf16[1,32,64,1408]{3,2,1,0:T(8,128)(2,1)}, bf16[1,32,64,1408]{3,2,1,0:T(8,128)(2,1)}) fusion(bf16[2,32,96,1408]{3,2,1,0:T(8,128)(2,1)} %bitcast.19), kind=kLoop, calls=%fused_computation.27 | loop fusion | bytes 23068672 | tf_op jit(solution)/shard_map/slice | solution.py:31
  134.2 0.0 collective-permute-done
  134.2 8.3 %fusion.15 = f32[512,1408]{1,0:T(8,128)} fusion(bf16[512,2048]{1,0:T(8,128)(2,1)} %collective-permute-done, bf16[2048,1408]{1,0:T(8,128)(2,1)} %bitcast.24), kind=kOutput, calls=%fused_computation.30 | convolution fusion | flops 2952790016 | bytes 10747904 | tf_op jit(solution)/shard_map/dot_general | solution.py:39
  142.5 13.9 %convolution_convert_fusion = bf16[512,2048]{1,0:T(8,128)(2,1)} fusion(bf16[2048,1408]{1,0:T(8,128)(2,1)} %bitcast.20, f32[512,1408]{1,0:T(8,128)} %fusion.15, bf16[512,2048]{1,0:T(8,128)(2,1)} %collective-permute-done, bf16[2048,1408]{1,0:T(8,128)(2,1)} %bitcast.22), kind=kOutput, calls=%fused_computation.16 | convolution fusion | flops 5910953984 | bytes 18612224 | tf_op jit(solution)/shard_map/dot_general | solution.py:42
  156.3 0.8 collective-permute-start.1
  157.2 0.0 copy-done.2
  157.2 8.3 %fusion.14 = f32[512,1408]{1,0:T(8,128)} fusion(bf16[512,2048]{1,0:T(8,128)(2,1)} %fusion.5, bf16[2048,1408]{1,0:T(8,128)(2,1)} %bitcast.25), kind=kOutput, calls=%fused_computation.29 | convolution fusion | flops 2952790016 | bytes 10747904 | tf_op jit(solution)/shard_map/dot_general | solution.py:39
  165.4 0.0 collective-permute-done.1
  165.4 14.5 %fusion = (f32[512]{0:T(512)S(1)}, bf16[512,2048]{1,0:T(8,128)(2,1)}) fusion(bf16[512,2048]{1,0:T(8,128)(2,1)} %collective-permute-done.1, bf16[2048,1408]{1,0:T(8,128)(2,1)} %bitcast.21, bf16[512,2048]{1,0:T(8,128)(2,1)} %fusion.5, bf16[2048,1408]{1,0:T(8,128)(2,1)} %bitcast.23, f32[512,1408]{1,0:T(8,128)} %fusion.14), kind=kOutput, calls=%fused_computation.6 | convolution fusion | flops 5918293504 | bytes 20711424 | tf_op jit(solution)/shard_map/dot_general | solution.py:42
  180.0 4.2 %fusion.6 = bf16[512,2048]{1,0:T(8,128)(2,1)} fusion(bf16[512,2048]{1,0:T(8,128)(2,1)} %get-tuple-element.8, bf16[512,2048]{1,0:T(8,128)(2,1)S(1)} %copy-done.1, f32[2048]{0:T(1024)S(1)} %convert_element_type.51, f32[512]{0:T(512)S(1)} %add_rsqrt_fusion), kind=kLoop, calls=%fused_computation.12 | loop fusion | flops 7340032 | bytes 6301696 | tf_op jit(solution)/shard_map/convert_element_type | solution.py:50
  (6 shorter events, 0.0 us)
Async XLA Ops:
  6.5 0.9 copy-start
  6.5 5.4 %copy-start.1 = (bf16[512,2048]{1,0:T(8,128)(2,1)S(1)}, bf16[512,2048]{1,0:T(8,128)(2,1)}, u32[]{:S(2)}) copy-start(bf16[512,2048]{1,0:T(8,128)(2,1)} %param.6) | copy-start | bytes 6291460
  6.5 111.9 %all-gather.3.cloned.1.call-start = ((), (), s32[]{:S(2)}) async-start(), calls=%async_computation | async-start | bytes 17571840 | tf_op jit(solution)/shard_map/all_gather | solution.py:29
  13.8 120.4 %collective-permute-start = (bf16[512,2048]{1,0:T(8,128)(2,1)}, bf16[512,2048]{1,0:T(8,128)(2,1)}, u32[]{:S(2)}, u32[]{:S(2)}) collective-permute-start(bf16[512,2048]{1,0:T(8,128)(2,1)} %fusion.5), channel_id=1, source_target_pairs={{0,1},{1,0},{2,3},{3,2},{4,5},{5,4},{6,7},{7,6},{8,9},{9,8},{10,11... | collective-permute-start | bytes 6291464 | tf_op jit(solution)/shard_map/ppermute | solution.py:36
  142.5 14.7 %copy-start.2 = (bf16[2048]{0:T(1024)(128)(2,1)S(1)}, bf16[2048]{0:T(1024)(128)(2,1)}, u32[]{:S(2)}) copy-start(bf16[2048]{0:T(1024)(128)(2,1)} %param.11) | copy-start | bytes 12292
  156.3 9.1 %collective-permute-start.1 = (bf16[512,2048]{1,0:T(8,128)(2,1)}, bf16[512,2048]{1,0:T(8,128)(2,1)}, u32[]{:S(2)}, u32[]{:S(2)}) collective-permute-start(bf16[512,2048]{1,0:T(8,128)(2,1)} %convolution_convert_fusion), channel_id=1, source_target_pairs={{0,1},{1,0},{2,3},{3,2},{4,5},{5,4},{6,7},{7,6},{8,9},{9,8},{10,11... | collective-permute-start | bytes 6291464 | tf_op jit(solution)/shard_map/ppermute | solution.py:46
Sparse Core Ops, SparseCore 0:
  10.1 108.2 all-gather.2
